TPU v7x, 32 devices: a whole 2x2x4 slice. The times are simulated.
32 devices in a mesh: grp: 2 (over x), fs: 4 (over z), tp: 4 (over y, core).
Axes of the slice: x: 2, y: 2, z: 4, core: 2. Of those that a mesh axis runs over, the one named last changes fastest.
Arguments:
- stream: bfloat16 [2048, 2048], P(('grp', 'fs'), 'tp'), parts along dimension 0, may hold values from -80 to 80
- mixed: bfloat16 [2048, 2048], P(('grp', 'fs'), 'tp'), parts along dimension 0, may hold values from -6 to 6
- out_weight: bfloat16 [2048, 2048], P('fs', 'tp'), may hold values from -0.125 to 0.125
- norm_gain: bfloat16 [2048], P('tp'), may hold values from 0.099609375 to 1.8984375
- up_weight: bfloat16 [2048, 8192], P('fs', 'tp'), may hold values from -0.125 to 0.125
- down_weight: bfloat16 [8192, 2048], P('tp', 'fs'), may hold values from -0.09375 to 0.09375
Outputs:
- result: bfloat16 [2048, 2048], P(('grp', 'fs'), 'tp'), parts along dimension 0
There are 2 independent parts, one for each index of `grp`. A program takes and returns all parts, laid end to end along the dimension named above; an argument that names none is the same for every part. Nothing has to cross between parts.
All inputs are finite; a program needn't handle non-finite values.
Results may differ from a plain program's by a relative error of at most 0.01.
Values may be sent and summed in bfloat16 or wider, within the bound.
A program may use at most 64 MiB of HBM per device.

v0:
```python
import jax
import jax.numpy as jnp
from jax import lax
from jax.sharding import PartitionSpec as P

epsilon = 1e-06


def fold_product(left, portion):
    return jnp.dot(left, portion, preferred_element_type=jnp.float32)


def body(stream, mixed, out_weight, norm_gain, up_weight, down_weight):
    mixed_whole = lax.all_gather(mixed, "tp", axis=1, tiled=True)
    projected = fold_product(mixed_whole, lax.all_gather(out_weight, "fs", axis=0, tiled=True))
    resid = (stream.astype(jnp.float32) + projected).astype(jnp.bfloat16)
    widened = resid.astype(jnp.float32)
    resid_whole, gain_whole = (
        lax.all_gather(resid, "tp", axis=1, tiled=True),
        lax.all_gather(norm_gain, "tp", axis=0, tiled=True),
    )
    stream_wide = resid_whole.astype(jnp.float32)
    energy = jnp.mean(stream_wide * stream_wide, axis=1, keepdims=True)
    normed_whole = (
        stream_wide * lax.rsqrt(energy + epsilon) * gain_whole.astype(jnp.float32)
    ).astype(jnp.bfloat16)
    up_full = lax.all_gather(up_weight, "fs", axis=0, tiled=True)
    up_values = jnp.dot(normed_whole, up_full, preferred_element_type=jnp.float32)
    activated = jnp.square(jax.nn.relu(up_values)).astype(jnp.bfloat16)
    partials = jnp.dot(
        activated,
        lax.all_gather(down_weight, "fs", axis=1, tiled=True),
        preferred_element_type=jnp.float32,
    )
    branch = lax.psum_scatter(partials, "tp", scatter_dimension=1, tiled=True)
    return (widened + branch).astype(jnp.bfloat16)


def solution(mesh):
    placed = (
        P(("grp", "fs"), "tp"),
        P(("grp", "fs"), "tp"),
        P("fs", "tp"),
        P("tp"),
        P("fs", "tp"),
        P("tp", "fs"),
    )
    return jax.shard_map(
        body, mesh=mesh, in_specs=placed, out_specs=P(("grp", "fs"), "tp"), check_vma=False
    )
```

profile of v0, /device:TPU:0, one launch (start us, length us, event | category | flops | bytes accessed | tf_op | source)
XLA Modules:
  0.0 445.1 jit_solution(17761984811447888567)
XLA Ops:
  6.5 0.0 all-gather.7.cloned.1.call-start
  6.5 0.7 all-gather.7.cloned.1.call-update
  7.3 0.0 all-gather.9.cloned.1.call-start
  7.3 0.7 all-gather.9.cloned.1.call-update
  8.0 0.0 all-gather.11.cloned.1.call-start
  8.1 20.3 %all-gather.7.cloned.1.call-done = bf16[256,2048]{1,0:T(8,128)(2,1)} async-done(((bf16[256,512]{1,0:T(8,128)(2,1)}), bf16[256,2048]{1,0:T(8,128)(2,1)}) %all-gather.7.cloned.1.call-update) | async-done | bytes 1048592 | tf_op jit(solution)/shard_map/all_gather | solution.py:14
  28.4 47.3 %all-gather.9.cloned.1.call-done = bf16[2048,512]{1,0:T(8,128)(2,1)} async-done(((bf16[512,512]{1,0:T(8,128)(2,1)}), bf16[2048,512]{1,0:T(8,128)(2,1)}) %all-gather.9.cloned.1.call-update) | async-done | bytes 2097168 | tf_op jit(solution)/shard_map/all_gather | solution.py:15
  75.6 3.3 fusion.5
  78.9 0.0 all-gather.11.cloned.1.call-update
  78.9 0.0 copy-start.1
  78.9 0.0 all-gather.13.cloned.1.call-start
  79.0 0.5 all-gather.13.cloned.1.call-update
  79.5 0.0 all-gather.15.cloned.1.call-start
  79.6 0.5 all-gather.15.cloned.1.call-update
  80.1 0.0 reduce-scatter.2.cloned.1.call-start
  80.2 0.0 copy-done.1
  80.2 5.2 %all-gather = bf16[4,1,512]{2,1,0:T(2,128)(2,1)S(1)} all-gather(bf16[1,1,512]{2,1,0:T(2,128)(2,1)S(1)} %reshape.9), channel_id=1, replica_groups=mesh['grp'=2,'fs'=4,'tp'=4] {'tp'}, dimensions={0}, use_global_device_ids=true | all-gather | bytes 5120 | tf_op jit(solution)/shard_map/all_gather | solution.py:20
  85.4 9.2 %all-gather.11.cloned.1.call-done = bf16[256,2048]{1,0:T(8,128)(2,1)} async-done(((bf16[256,512]{1,0:T(8,128)(2,1)}), bf16[256,2048]{1,0:T(8,128)(2,1)}) %all-gather.11.cloned.1.call-update) | async-done | bytes 1048592 | tf_op jit(solution)/shard_map/all_gather | solution.py:19
  94.6 1.5 fusion.2
  96.1 149.5 %all-gather.13.cloned.1.call-done = bf16[2048,2048]{1,0:T(8,128)(2,1)} async-done(((bf16[512,2048]{1,0:T(8,128)(2,1)}), bf16[2048,2048]{1,0:T(8,128)(2,1)}) %all-gather.13.cloned.1.call-update) | async-done | bytes 8388624 | tf_op jit(solution)/shard_map/all_gather | solution.py:27
  245.7 149.2 %all-gather.15.cloned.1.call-done = bf16[2048,2048]{1,0:T(8,128)(2,1)} async-done(((bf16[2048,512]{1,0:T(8,128)(2,1)}), bf16[2048,2048]{1,0:T(8,128)(2,1)}) %all-gather.15.cloned.1.call-update) | async-done | bytes 8388624 | tf_op jit(solution)/shard_map/all_gather | solution.py:32
  394.9 11.9 %fusion.10 = f32[256,2048]{1,0:T(8,128)} fusion(bf16[2048,2048]{1,0:T(8,128)(2,1)} %all-gather.15.cloned.1.call-done, bf16[2048,2048]{1,0:T(8,128)(2,1)} %all-gather.13.cloned.1.call-done, bf16[256,2048]{1,0:T(8,128)(2,1)} %all-gather.11.cloned.1.call-done, f32[2048]{0:T(1024)S(1)} %bitcast.5, f32[256]{0:T(256)S(1)} %add_rsqrt_fusion), kind=kOutput, calls=%fused_computation.12 | convolution fusion | flops 4298637312 | bytes 19932160 | tf_op jit(solution)/shard_map/dot_general | solution.py:30
  406.9 0.0 copy-start
  406.9 0.0 reduce-scatter.2.cloned.1.call-update
  406.9 29.5 %reduce-scatter.2.cloned.1.call-done = f32[256,512]{1,0:T(8,128)} async-done(((f32[256,2048]{1,0:T(8,128)}), f32[256,512]{1,0:T(8,128)}) %reduce-scatter.2.cloned.1.call-update) | async-done | bytes 524304 | tf_op jit(solution)/shard_map/reduce_scatter | solution.py:35
  436.4 0.0 copy-done
  436.4 1.8 add_convert_fusion
  (3 shorter events, 0.0 us)
Async XLA Ops:
  6.5 21.8 %all-gather.7.cloned.1.call-start = ((), (), s32[]{:S(2)}) async-start(), calls=%async_computation.1 | async-start | bytes 1310720 | tf_op jit(solution)/shard_map/all_gather | solution.py:14
  7.3 68.3 %all-gather.9.cloned.1.call-start = ((), (), s32[]{:S(2)}) async-start(), calls=%async_computation.2 | async-start | bytes 2621440 | tf_op jit(solution)/shard_map/all_gather | solution.py:15
  8.0 86.6 %all-gather.11.cloned.1.call-start = ((), (), s32[]{:S(2)}) async-start(), calls=%async_computation.3 | async-start | bytes 1310720 | tf_op jit(solution)/shard_map/all_gather | solution.py:19
  78.9 1.2 copy-start.1
  78.9 166.7 %all-gather.13.cloned.1.call-start = ((), (), s32[]{:S(2)}) async-start(), calls=%async_computation.4 | async-start | bytes 10485760 | tf_op jit(solution)/shard_map/all_gather | solution.py:27
  79.5 315.4 %all-gather.15.cloned.1.call-start = ((), (), s32[]{:S(2)}) async-start(), calls=%async_computation.5 | async-start | bytes 10485760 | tf_op jit(solution)/shard_map/all_gather | solution.py:32
  80.1 356.3 %reduce-scatter.2.cloned.1.call-start = ((), (), s32[]{:S(2)}) async-start(), calls=%async_computation.6 | async-start | bytes 2621440 | tf_op jit(solution)/shard_map/reduce_scatter | solution.py:35
  406.9 29.6 %copy-start = (bf16[256,512]{1,0:T(8,128)(2,1)S(1)}, bf16[256,512]{1,0:T(8,128)(2,1)}, u32[]{:S(2)}) copy-start(bf16[256,512]{1,0:T(8,128)(2,1)} %fusion.5) | copy-start | bytes 786436
Sparse Core Ops, SparseCore 0:
  8.9 19.4 all-gather.6
  29.9 45.6 all-gather.8
  79.1 15.4 all-gather.10
  96.0 149.5 all-gather.12
  247.1 147.7 all-gather.14
  407.0 29.3 reduce-scatter.1
where the time goes:
time: 445 us
  waiting for transfers between devices  408 us (92%)
  matrix products  15.3 us (3%)
  between operations  13.5 us (3%)
  blocking collectives  5.19 us (1%)
    all_gather x1, waiting for transfers between devices, body(): up_full = lax.all_gather(up_weight, 'fs', axis=0, tiled=True)  150 us
    all_gather x1, waiting for transfers between devices, body(): lax.all_gather(down_weight, 'fs', axis=1, tiled=True)  149 us
    all_gather x1, waiting for transfers between devices, body(): lax.all_gather(out_weight, 'fs', axis=0, tiled=True)  47.3 us
    reduce_scatter x1, waiting for transfers between devices, body(): branch = lax.psum_scatter(partials, 'tp', scatter_dimension=1, tiled=True)  29.5 us
    all_gather x1, waiting for transfers between devices, body(): mixed_whole = lax.all_gather(mixed, 'tp', axis=1, tiled=True)  20.3 us
    dot_general x1, matrix products, body(): jnp.dot(activated, lax.all_gather(down_weight, 'fs', axis=1, tiled=True),...  11.9 us
    all_gather x1, waiting for transfers between devices, body(): lax.all_gather(resid, 'tp', axis=1, tiled=True)  9.21 us
  transfers between devices with their start and end apart: 6, of which 6 were waited for; matrix products, arithmetic and copies ran while one was open for 0% of the time, Pallas kernels for 0%

commit v1 on v0

--- a/solution.py
+++ b/solution.py
@@ -24,7 +24,12 @@
     normed_whole = (
         stream_wide * lax.rsqrt(energy + epsilon) * gain_whole.astype(jnp.float32)
     ).astype(jnp.bfloat16)
-    up_full = lax.all_gather(up_weight, "fs", axis=0, tiled=True)
+    ring = [up_weight]
+    for hop in range(3):
+        ring.append(lax.ppermute(ring[-1], "fs", [(dev, (dev + 1) % 4) for dev in range(4)]))
+    up_full = jnp.roll(
+        jnp.concatenate(ring[::-1], axis=0), (lax.axis_index("fs") + 1) * ring[0].shape[0], axis=0
+    )
     up_values = jnp.dot(normed_whole, up_full, preferred_element_type=jnp.float32)
     activated = jnp.square(jax.nn.relu(up_values)).astype(jnp.bfloat16)
     partials = jnp.dot(

time: 445 us -> 423 us (0.951)
  waiting for transfers between devices: 408 us -> 294 us
  starting transfers between devices: 0.2 us -> 70.3 us
  local copies, waits for them, and re-layouts: 0.01 us -> 21 us
    ppermute x0 -> x3, waiting for transfers between devices: none -> 195 us  [body(): lax.ppermute(ring[-1], 'fs', [(dev, (dev + 1) % 4) for dev in range(4)])]
    all_gather x1 -> x0, waiting for transfers between devices: 150 us -> none  [body(): up_full = lax.all_gather(up_weight, 'fs', axis=0, tiled=True)]
    all_gather x1, waiting for transfers between devices: 149 us -> 0.01 us  [body(): lax.all_gather(down_weight, 'fs', axis=1, tiled=True)]
    ppermute x0 -> x3, starting transfers between devices: none -> 70.1 us  [body(): lax.ppermute(ring[-1], 'fs', [(dev, (dev + 1) % 4) for dev in range(4)])]
    unnamed x5 -> x18, local copies, waits for them, and re-layouts: 0.01 us -> 19.4 us
    all_gather x1, waiting for transfers between devices: 9.21 us -> 0.02 us  [body(): lax.all_gather(resid, 'tp', axis=1, tiled=True)]
  transfers between devices with their start and end apart: 6 -> 8, of which waited for: 6 -> 6; matrix products, arithmetic and copies ran while one was open for 0% -> 5% of each run, Pallas kernels for 0% -> 0%
where the time goes in v1:
time: 423 us
  waiting for transfers between devices  294 us (70%)
  starting transfers between devices  70.3 us (17%)
  local copies, waits for them, and re-layouts  21 us (5%)
  matrix products  15.1 us (4%)
  between operations  13.2 us (3%)
  blocking collectives  5.18 us (1%)
    ppermute x3, waiting for transfers between devices, body(): lax.ppermute(ring[-1], 'fs', [(dev, (dev + 1) % 4) for dev in range(4)])  195 us
    ppermute x3, starting transfers between devices, body(): lax.ppermute(ring[-1], 'fs', [(dev, (dev + 1) % 4) for dev in range(4)])  70.1 us
    all_gather x1, waiting for transfers between devices, body(): lax.all_gather(out_weight, 'fs', axis=0, tiled=True)  47.3 us
    reduce_scatter x1, waiting for transfers between devices, body(): branch = lax.psum_scatter(partials, 'tp', scatter_dimension=1, tiled=True)  29.5 us
    all_gather x1, waiting for transfers between devices, body(): mixed_whole = lax.all_gather(mixed, 'tp', axis=1, tiled=True)  20.3 us
    unnamed x18, local copies, waits for them, and re-layouts  19.4 us
    dot_general x1, matrix products, body(): jnp.dot(activated, lax.all_gather(down_weight, 'fs', axis=1, tiled=True),...  11.8 us
  transfers between devices with their start and end apart: 8, of which 6 were waited for; matrix products, arithmetic and copies ran while one was open for 5% of the time, Pallas kernels for 0%

profile of v1, /device:TPU:0, one launch (start us, length us, event | category | flops | bytes accessed | tf_op | source)
XLA Modules:
  0.0 422.6 jit_solution(14289356904373567895)
XLA Ops:
  6.5 0.7 all-gather.6.cloned.1.call-update
  7.3 0.0 all-gather.8.cloned.1.call-start
  7.3 0.7 all-gather.8.cloned.1.call-update
  8.0 0.0 all-gather.10.cloned.1.call-start
  8.1 20.3 %all-gather.6.cloned.1.call-done = bf16[256,2048]{1,0:T(8,128)(2,1)} async-done(((bf16[256,512]{1,0:T(8,128)(2,1)}), bf16[256,2048]{1,0:T(8,128)(2,1)}) %all-gather.6.cloned.1.call-update) | async-done | bytes 1048592 | tf_op jit(solution)/shard_map/all_gather | solution.py:14
  28.4 47.3 %all-gather.8.cloned.1.call-done = bf16[2048,512]{1,0:T(8,128)(2,1)} async-done(((bf16[512,512]{1,0:T(8,128)(2,1)}), bf16[2048,512]{1,0:T(8,128)(2,1)}) %all-gather.8.cloned.1.call-update) | async-done | bytes 2097168 | tf_op jit(solution)/shard_map/all_gather | solution.py:15
  75.6 3.3 fusion.14
  78.9 0.0 all-gather.12.cloned.1.call-start
  79.0 0.5 all-gather.12.cloned.1.call-update
  79.5 0.0 reduce-scatter.2.cloned.1.call-start
  79.6 0.2 collective-permute-start
  79.8 69.2 %collective-permute-done = bf16[512,2048]{1,0:T(8,128)(2,1)S(1)} collective-permute-done((bf16[512,2048]{1,0:T(8,128)(2,1)}, bf16[512,2048]{1,0:T(8,128)(2,1)S(1)}, u32[]{:S(2)}, u32[]{:S(2)}) %collective-permute-start) | collective-permute-done | bytes 2097184 | tf_op jit(solution)/shard_map/ppermute | solution.py:29
  149.0 1.4 copy-done.1
  150.3 20.1 %collective-permute-start.1 = (bf16[512,2048]{1,0:T(8,128)(2,1)S(1)}, bf16[512,2048]{1,0:T(8,128)(2,1)}, u32[]{:S(2)}, u32[]{:S(2)}) collective-permute-start(bf16[512,2048]{1,0:T(8,128)(2,1)S(1)} %collective-permute-done), channel_id=1, source_target_pairs={{0,4},{4,8},{8,12},{12,0},{1,5},{5,9},{9,13},{13,1},{2,6},{6,10},{... | collective-permute-start | bytes 6291464 | tf_op jit(solution)/shard_map/ppermute | solution.py:29
  170.4 87.3 %collective-permute-done.1 = bf16[512,2048]{1,0:T(8,128)(2,1)} collective-permute-done((bf16[512,2048]{1,0:T(8,128)(2,1)S(1)}, bf16[512,2048]{1,0:T(8,128)(2,1)}, u32[]{:S(2)}, u32[]{:S(2)}) %collective-permute-start.1) | collective-permute-done | bytes 2097184 | tf_op jit(solution)/shard_map/ppermute | solution.py:29
  257.7 49.8 %collective-permute-start.2 = (bf16[512,2048]{1,0:T(8,128)(2,1)}, bf16[512,2048]{1,0:T(8,128)(2,1)}, u32[]{:S(2)}, u32[]{:S(2)}) collective-permute-start(bf16[512,2048]{1,0:T(8,128)(2,1)} %collective-permute-done.1), channel_id=1, source_target_pairs={{0,4},{4,8},{8,12},{12,0},{1,5},{5,9},{9,13},{13,1},{2,6},{6,10},{... | collective-permute-start | bytes 6291464 | tf_op jit(solution)/shard_map/ppermute | solution.py:29
  307.5 0.7 reshape.9
  308.2 5.2 %all-gather = bf16[4,1,512]{2,1,0:T(2,128)(2,1)S(1)} all-gather(bf16[1,1,512]{2,1,0:T(2,128)(2,1)S(1)} %reshape.9), channel_id=1, replica_groups=mesh['grp'=2,'fs'=4,'tp'=4] {'tp'}, dimensions={0}, use_global_device_ids=true | all-gather | bytes 5120 | tf_op jit(solution)/shard_map/all_gather | solution.py:20
  313.4 0.0 all-gather.10.cloned.1.call-done
  313.5 1.7 fusion.11
  315.1 38.9 %collective-permute-done.2 = bf16[512,2048]{1,0:T(8,128)(2,1)} collective-permute-done((bf16[512,2048]{1,0:T(8,128)(2,1)}, bf16[512,2048]{1,0:T(8,128)(2,1)}, u32[]{:S(2)}, u32[]{:S(2)}) %collective-permute-start.2) | collective-permute-done | bytes 2097184 | tf_op jit(solution)/shard_map/ppermute | solution.py:29
  354.0 3.2 constant_dynamic-update-slice_fusion.7
  357.2 3.2 constant_dynamic-update-slice_fusion.6
  360.3 1.5 constant_dynamic-update-slice_fusion.5
  361.8 1.6 constant_dynamic-update-slice_fusion.4
  363.4 3.3 constant_dynamic-update-slice_fusion.3
  366.7 3.2 constant_dynamic-update-slice_fusion.2
  369.9 1.5 constant_dynamic-update-slice_fusion.1
  371.4 1.6 constant_dynamic-update-slice_fusion
  373.0 11.8 %fusion.20 = f32[256,2048]{1,0:T(8,128)} fusion(bf16[2048,2048]{1,0:T(8,128)(2,1)} %all-gather.12.cloned.1.call-done, bf16[4096,2048]{1,0:T(8,128)(2,1)} %constant_dynamic-update-slice_fusion, s32[]{:T(128)S(6)} %select_n.14, bf16[256,2048]{1,0:T(8,128)(2,1)S(1)} %copy-done.3, f32[2048]{0:T(1024)S(1)} %bitcast.4, f32[256]{0:T(256)S(1)} %add_rsqrt_fusion), kind=kOutput, calls=%fused_computation.14 | convolution fusion | flops 4298637312 | bytes 19932164 | tf_op jit(solution)/shard_map/dot_general | solution.py:35
  384.7 29.5 %reduce-scatter.2.cloned.1.call-done = f32[256,512]{1,0:T(8,128)} async-done(((f32[256,2048]{1,0:T(8,128)}), f32[256,512]{1,0:T(8,128)}) %reduce-scatter.2.cloned.1.call-update) | async-done | bytes 524304 | tf_op jit(solution)/shard_map/reduce_scatter | solution.py:40
  414.2 1.8 add_convert_fusion
  (15 shorter events, 0.1 us)
Async XLA Ops:
  6.5 21.8 %all-gather.6.cloned.1.call-start = ((), (), s32[]{:S(2)}) async-start(), calls=%async_computation.1 | async-start | bytes 1310720 | tf_op jit(solution)/shard_map/all_gather | solution.py:14
  7.3 68.3 %all-gather.8.cloned.1.call-start = ((), (), s32[]{:S(2)}) async-start(), calls=%async_computation.2 | async-start | bytes 2621440 | tf_op jit(solution)/shard_map/all_gather | solution.py:15
  8.0 305.4 %all-gather.10.cloned.1.call-start = ((), (), s32[]{:S(2)}) async-start(), calls=%async_computation.3 | async-start | bytes 1310720 | tf_op jit(solution)/shard_map/all_gather | solution.py:19
  78.9 282.9 %copy-start = (bf16[512,2048]{1,0:T(8,128)(2,1)S(1)}, bf16[512,2048]{1,0:T(8,128)(2,1)}, u32[]{:S(2)}) copy-start(bf16[512,2048]{1,0:T(8,128)(2,1)} %param.10) | copy-start | bytes 6291460
  78.9 294.0 %all-gather.12.cloned.1.call-start = ((), (), s32[]{:S(2)}) async-start(), calls=%async_computation.4 | async-start | bytes 10485760 | tf_op jit(solution)/shard_map/all_gather | solution.py:37
  79.5 334.7 %reduce-scatter.2.cloned.1.call-start = ((), (), s32[]{:S(2)}) async-start(), calls=%async_computation.5 | async-start | bytes 2621440 | tf_op jit(solution)/shard_map/reduce_scatter | solution.py:40
  79.6 69.4 %collective-permute-start = (bf16[512,2048]{1,0:T(8,128)(2,1)}, bf16[512,2048]{1,0:T(8,128)(2,1)S(1)}, u32[]{:S(2)}, u32[]{:S(2)}) collective-permute-start(bf16[512,2048]{1,0:T(8,128)(2,1)} %param.10), channel_id=1, source_target_pairs={{0,4},{4,8},{8,12},{12,0},{1,5},{5,9},{9,13},{13,1},{2,6},{6,10},{... | collective-permute-start | bytes 6291464 | tf_op jit(solution)/shard_map/ppermute | solution.py:29
  149.0 1.4 copy-start.1
  150.3 107.4 %collective-permute-start.1 = (bf16[512,2048]{1,0:T(8,128)(2,1)S(1)}, bf16[512,2048]{1,0:T(8,128)(2,1)}, u32[]{:S(2)}, u32[]{:S(2)}) collective-permute-start(bf16[512,2048]{1,0:T(8,128)(2,1)S(1)} %collective-permute-done), channel_id=1, source_target_pairs={{0,4},{4,8},{8,12},{12,0},{1,5},{5,9},{9,13},{13,1},{2,6},{6,10},{... | collective-permute-start | bytes 6291464 | tf_op jit(solution)/shard_map/ppermute | solution.py:29
  257.7 96.3 %collective-permute-start.2 = (bf16[512,2048]{1,0:T(8,128)(2,1)}, bf16[512,2048]{1,0:T(8,128)(2,1)}, u32[]{:S(2)}, u32[]{:S(2)}) collective-permute-start(bf16[512,2048]{1,0:T(8,128)(2,1)} %collective-permute-done.1), channel_id=1, source_target_pairs={{0,4},{4,8},{8,12},{12,0},{1,5},{5,9},{9,13},{13,1},{2,6},{6,10},{... | collective-permute-start | bytes 6291464 | tf_op jit(solution)/shard_map/ppermute | solution.py:29
  313.4 46.9 %copy-start.2 = (bf16[512,2048]{1,0:T(8,128)(2,1)S(1)}, bf16[512,2048]{1,0:T(8,128)(2,1)}, u32[]{:S(2)}) copy-start(bf16[512,2048]{1,0:T(8,128)(2,1)} %copy-done.1) | copy-start | bytes 6291460
  363.4 9.5 %copy-start.3 = (bf16[256,2048]{1,0:T(8,128)(2,1)S(1)}, bf16[256,2048]{1,0:T(8,128)(2,1)}, u32[]{:S(2)}) copy-start(bf16[256,2048]{1,0:T(8,128)(2,1)} %all-gather.10.cloned.1.call-done) | copy-start | bytes 3145732
  373.0 41.3 %copy-start.4 = (bf16[256,512]{1,0:T(8,128)(2,1)S(1)}, bf16[256,512]{1,0:T(8,128)(2,1)}, u32[]{:S(2)}) copy-start(bf16[256,512]{1,0:T(8,128)(2,1)} %fusion.14) | copy-start | bytes 786436
Sparse Core Ops, SparseCore 0:
  8.9 19.4 all-gather.5
  29.9 45.6 all-gather.7
  79.1 15.4 all-gather.9
  96.0 216.7 all-gather.11
  384.9 29.3 reduce-scatter.1
